TPU v7x, 32 devices: a whole 2x2x4 slice. The times are simulated.
32 devices in a mesh: ep: 16 (over z, y, x), tp: 2 (over core).
Axes of the slice: x: 2, y: 2, z: 4, core: 2. Of those that a mesh axis runs over, the one named last changes fastest.
Arguments:
- tokens: bfloat16 [256, 1536], P('ep'), may hold values from -6 to 6
- prior_state: float32 [256, 12, 64, 64], P('ep', 'tp'), may hold values from -12 to 12
- first_gain: float32 [1536], replicated, may hold values from 0.1 to 1.9
- query_weight: bfloat16 [1536, 768], P(None, 'tp'), may hold values from -0.15625 to 0.15625
- key_weight: bfloat16 [1536, 768], P(None, 'tp'), may hold values from -0.15625 to 0.15625
- value_weight: bfloat16 [1536, 768], P(None, 'tp'), may hold values from -0.15625 to 0.15625
- decay_down: bfloat16 [1536, 96], replicated, may hold values from -0.15625 to 0.15625
- decay_up: bfloat16 [96, 768], P(None, 'tp'), may hold values from -1.25 to 1.25
- decay_base: float32 [768], P('tp'), may hold values from -5 to 1
- rate_down: bfloat16 [1536, 96], replicated, may hold values from -0.15625 to 0.15625
- rate_up: bfloat16 [96, 768], P(None, 'tp'), may hold values from -1.25 to 1.25
- rate_base: float32 [768], P('tp'), may hold values from -4 to 4
- head_gain: float32 [768], P('tp'), may hold values from 0.1 to 1.9
- out_weight: bfloat16 [768, 1536], P('tp'), may hold values from -0.21875 to 0.21875
- mid_gain: float32 [1536], replicated, may hold values from 0.1 to 1.9
- route_ids: int32 [256, 6], P('ep'), may hold values from 0 to 15, all different within a row; in each aligned block of 16 rows (0 to 15, 16 to 31, ...) at most 12 rows name the same one
- route_weights: float32 [256, 6], P('ep'), may hold values from 0.1 to 1
- expert_gate: bfloat16 [16, 1536, 384], P('ep', None, 'tp'), may hold values from -0.15625 to 0.15625
- expert_up: bfloat16 [16, 1536, 384], P('ep', None, 'tp'), may hold values from -0.15625 to 0.15625
- expert_down: bfloat16 [16, 384, 1536], P('ep', 'tp'), may hold values from -0.3125 to 0.3125
- dense_gate: bfloat16 [1536, 6144], P(None, ('ep', 'tp')), may hold values from -0.15625 to 0.15625
- dense_up: bfloat16 [1536, 6144], P(None, ('ep', 'tp')), may hold values from -0.15625 to 0.15625
- dense_down: bfloat16 [6144, 1536], P(('ep', 'tp')), may hold values from -0.078125 to 0.078125
- blend_vector: bfloat16 [1536], replicated, may hold values from -0.15625 to 0.15625
Outputs:
- mixed: bfloat16 [256, 1536], P('ep', 'tp')
- new_state: float32 [256, 12, 64, 64], P('ep', 'tp')
Inputs may be any that keep to these rules, and one draw needn't show every extreme that they name: `route_ids`: each row names 6 different experts; among the rows of one device no expert is named by more than 12 rows, a bound that some block reaches.
All inputs are finite; a program needn't handle non-finite values.
Results may differ from a plain program's by a relative error of at most 0.02.
Values may be sent and summed in bfloat16 or wider, within the bound.
A program may use at most 128 MiB of HBM per device.

v0:
```python
import jax
import jax.numpy as jnp
from jax import lax
from jax.sharding import PartitionSpec as P


def rms_norm(values, gain):
    scale = lax.rsqrt(jnp.mean(values * values, axis=-1, keepdims=True) + 1e-06)
    return values * scale * gain


def rounded(values):
    return lax.optimization_barrier(values.astype(jnp.bfloat16)).astype(jnp.float32)


def mixer_core(
    normed,
    prior_state,
    query_weight,
    key_weight,
    value_weight,
    decay_down,
    decay_up,
    decay_base,
    rate_down,
    rate_up,
    rate_base,
    head_gain,
):
    rows = normed.shape[0]
    heads_here = prior_state.shape[1]
    head_size = prior_state.shape[2]

    def project(weight):
        product = jnp.dot(normed, weight, preferred_element_type=jnp.float32)
        return rounded(product).reshape(rows, heads_here, head_size)

    receptance = project(query_weight)
    key_vec = project(key_weight)
    value_vec = project(value_weight)
    decay_low = jnp.tanh(jnp.dot(normed, decay_down, preferred_element_type=jnp.float32)).astype(
        jnp.bfloat16
    )
    decay_log = decay_base + jnp.dot(decay_low, decay_up, preferred_element_type=jnp.float32)
    decay_log = -jax.nn.softplus(-decay_log) - 0.5
    decay_rate = jnp.exp(-jnp.exp(decay_log)).reshape(rows, heads_here, head_size)
    rate_low = jnp.dot(normed, rate_down, preferred_element_type=jnp.float32).astype(jnp.bfloat16)
    learn_rate = jax.nn.sigmoid(
        rate_base + jnp.dot(rate_low, rate_up, preferred_element_type=jnp.float32)
    )
    learn_rate = learn_rate.reshape(rows, heads_here, head_size)
    unit_key = key_vec * lax.rsqrt(jnp.sum(key_vec * key_vec, axis=-1, keepdims=True) + 1e-06)
    removed = jnp.sum(prior_state * unit_key[:, :, None, :], axis=-1)
    new_state = (
        prior_state * decay_rate[:, :, None, :]
        - removed[..., None] * (unit_key * learn_rate)[:, :, None, :]
        + value_vec[..., None] * key_vec[:, :, None, :]
    )
    read = jnp.sum(new_state * receptance[:, :, None, :], axis=-1)
    center = jnp.mean(read, axis=-1, keepdims=True)
    spread = jnp.mean(jnp.square(read - center), axis=-1, keepdims=True)
    normal = (read - center) * lax.rsqrt(spread + 0.00064)
    mixed_heads = (normal.reshape(rows, -1) * head_gain).astype(jnp.bfloat16)
    return (mixed_heads, new_state)


def shards(
    tokens,
    prior_state,
    first_gain,
    query_weight,
    key_weight,
    value_weight,
    decay_down,
    decay_up,
    decay_base,
    rate_down,
    rate_up,
    rate_base,
    head_gain,
    out_weight,
    mid_gain,
    route_ids,
    route_weights,
    expert_gate,
    expert_up,
    expert_down,
    dense_gate,
    dense_up,
    dense_down,
    blend_vector,
):
    count_ep = lax.axis_size("ep")
    count_tp = lax.axis_size("tp")
    seqs = tokens.shape[0]
    width = tokens.shape[1]
    top_count = route_ids.shape[1]
    half_width = width // count_tp
    capacity = max(2, 2 * seqs * top_count // count_ep)
    token_f = tokens.astype(jnp.float32)
    normed = rms_norm(token_f, first_gain).astype(jnp.bfloat16)
    mixed_heads, new_state = mixer_core(
        normed,
        prior_state,
        query_weight,
        key_weight,
        value_weight,
        decay_down,
        decay_up,
        decay_base,
        rate_down,
        rate_up,
        rate_base,
        head_gain,
    )
    partial_value = jnp.dot(mixed_heads, out_weight, preferred_element_type=jnp.float32)
    attn = lax.psum(partial_value.astype(jnp.bfloat16), "tp").astype(jnp.float32)
    resid = rounded(token_f + attn)
    mid = rms_norm(resid, mid_gain).astype(jnp.bfloat16)
    blend = jax.nn.sigmoid(jnp.dot(mid, blend_vector, preferred_element_type=jnp.float32))
    flat_ids = route_ids.reshape(-1)
    onehot = (flat_ids[:, None] == jnp.arange(count_ep, dtype=jnp.int32)[None, :]).astype(jnp.int32)
    before = jnp.cumsum(onehot, axis=0) - onehot
    position = jnp.sum(onehot * before, axis=1)
    slot = flat_ids * capacity + position
    send = (
        jnp.zeros((count_ep * capacity, width), jnp.bfloat16)
        .at[slot]
        .set(jnp.repeat(mid, top_count, axis=0))
    )
    send = send.reshape(count_ep, capacity, width)
    gate_w = expert_gate[0]
    up_w = expert_up[0]
    down_w = expert_down[0]
    arrived = lax.all_to_all(send, "ep", split_axis=0, concat_axis=0, tiled=True)
    senders = arrived.shape[0]
    items = arrived.shape[1]
    rows_in = arrived.reshape(-1, width)
    hidden = (
        jax.nn.silu(jnp.dot(rows_in, gate_w, preferred_element_type=jnp.float32))
        * jnp.dot(rows_in, up_w, preferred_element_type=jnp.float32)
    ).astype(jnp.bfloat16)
    partial_out = jnp.dot(hidden, down_w, preferred_element_type=jnp.float32)
    summed = lax.psum_scatter(
        partial_out.astype(jnp.bfloat16), "tp", scatter_dimension=1, tiled=True
    )
    result = summed.reshape(senders, items, half_width)
    back = lax.all_to_all(result, "ep", split_axis=0, concat_axis=0, tiled=True)
    picked = (
        back.reshape(-1, half_width)[slot].astype(jnp.float32).reshape(seqs, top_count, half_width)
    )
    share = route_weights / jnp.sum(route_weights, axis=1, keepdims=True) * 2.5
    routed = jnp.sum(share[..., None] * picked, axis=1)
    piece = lax.all_gather(mid, "ep", axis=0, tiled=True)
    hidden_all = (
        jax.nn.silu(jnp.dot(piece, dense_gate, preferred_element_type=jnp.float32))
        * jnp.dot(piece, dense_up, preferred_element_type=jnp.float32)
    ).astype(jnp.bfloat16)
    term = jnp.einsum(
        "esf,ftd->etsd",
        hidden_all.reshape(count_ep, seqs, -1),
        dense_down.reshape(-1, count_tp, half_width),
        preferred_element_type=jnp.float32,
    )
    term = term.reshape(count_ep * count_tp, seqs, half_width)
    dense_out = lax.psum_scatter(term, ("ep", "tp"), scatter_dimension=0, tiled=True)[0]
    own_cols = lax.dynamic_slice_in_dim(resid, lax.axis_index("tp") * half_width, half_width, 1)
    mixed = (own_cols + routed + blend[:, None] * dense_out).astype(jnp.bfloat16)
    return (mixed, new_state)


def solution(mesh):
    in_specs = (
        P("ep", None),
        P("ep", "tp", None, None),
        P(),
        P(None, "tp"),
        P(None, "tp"),
        P(None, "tp"),
        P(),
        P(None, "tp"),
        P("tp"),
        P(),
        P(None, "tp"),
        P("tp"),
        P("tp"),
        P("tp", None),
        P(),
        P("ep", None),
        P("ep", None),
        P("ep", None, "tp"),
        P("ep", None, "tp"),
        P("ep", "tp", None),
        P(None, ("ep", "tp")),
        P(None, ("ep", "tp")),
        P(("ep", "tp"), None),
        P(),
    )
    out_specs = (P("ep", "tp"), P("ep", "tp", None, None))
    return jax.shard_map(shards, mesh=mesh, in_specs=in_specs, out_specs=out_specs, check_vma=False)
```

profile of v0, /device:TPU:0, one launch (start us, length us, event | category | flops | bytes accessed | tf_op | source)
XLA Modules:
  0.0 219.4 jit_solution(10005779780720382607)
XLA Ops:
  7.3 0.8 broadcast_multiply_fusion.2
  8.1 0.8 copy.33
  8.9 0.9 fusion.31
  9.8 1.6 convolution_convert_fusion.2
  11.6 1.6 convolution_convert_fusion.4
  13.3 1.6 convolution_convert_fusion.3
  15.1 0.4 fusion.10
  15.7 0.4 fusion.43
  16.3 15.7 %multiply_reduce_fusion.1 = (f32[16,6]{1,0:T(8,128)S(1)}, f32[16,6,64]{2,1,0:T(8,128)S(1)}, f32[16,6,64,64]{3,2,1,0:T(8,128)}) fusion(f32[16,6,64]{2,1,0:T(8,128)S(1)} %reshape.151, f32[16,6,64]{2,1,0:T(8,128)S(1)} %reshape.149, f32[16,6,64]{2,1,0:T(8,128)S(1)} %reshape.150, f32[16,6,64]{2,1,0:T(8,128)S(1)} %get-tuple-element.4, ...), kind=kOutput, calls=%fused_computation.6 | output fusion | flops 3538911 | bytes 3318144 | tf_op jit(solution)/shard_map/mul | solution.py:56
  32.6 3.8 %psum.7 = bf16[16,1536]{1,0:T(8,128)(2,1)S(1)} all-reduce(bf16[16,1536]{1,0:T(8,128)(2,1)S(1)} %convolution_convert_fusion.1), channel_id=1, replica_groups=mesh['ep'=16,'tp'=2] {'tp'}, use_global_device_ids=true, to_apply=%region_6.7 | all-reduce | flops 24576 | bytes 98304 | tf_op jit(solution)/shard_map/psum | solution.py:117
  37.6 1.2 scatter_custom_fusion
  39.0 29.6 %all_to_all.10 = bf16[16,12,1536]{2,1,0:T(8,128)(2,1)S(1)} all-to-all(bf16[16,12,1536]{2,1,0:T(8,128)(2,1)S(1)} %reshape.141), channel_id=1, replica_groups=mesh['ep'=16,'tp'=2] {'ep'}, dimensions={0} | all-to-all | bytes 1179648 | tf_op jit(solution)/shard_map/all_to_all | solution.py:135
  68.7 0.3 fusion.22
  69.1 3.0 %convolution_convert_fusion = bf16[192,1536]{1,0:T(8,128)(2,1)} fusion(bf16[192,1536]{1,0:T(8,128)(2,1)S(1)} %reshape.142, bf16[1,192,1536]{2,1,0:T(8,128)(2,1)} %param.43, bf16[1,1536,192]{1,2,0:T(8,128)(2,1)} %param.42, f32[192,192]{1,0:T(8,128)S(1)} %fusion.22), kind=kOutput, calls=%fused_computation.8 | convolution fusion | flops 227008512 | bytes 2506752 | tf_op jit(solution)/shard_map/dot_general | solution.py:143
  72.1 42.2 %all_gather.3 = bf16[256,1536]{1,0:T(8,128)(2,1)S(1)} all-gather(bf16[16,1536]{1,0:T(8,128)(2,1)S(1)} %multiply_convert_fusion), channel_id=1, replica_groups=mesh['ep'=16,'tp'=2] {'ep'}, dimensions={0}, use_global_device_ids=true | all-gather | bytes 835584 | tf_op jit(solution)/shard_map/all_gather | solution.py:154
  114.4 0.4 fusion.55
  114.8 0.4 fusion.6
  115.3 1.5 fusion.17
  117.0 1.8 reshape.143
  118.7 3.6 %all-to-all-start.1 = ((bf16[16,12,768]{2,1,0:T(8,128)(2,1)}), bf16[16,12,768]{2,1,0:T(8,128)(2,1)S(1)}, u32[]{:S(2)}, u32[]{:S(2)}) async-start(bf16[16,12,768]{2,1,0:T(8,128)(2,1)} %reshape.143), calls=%async_computation.2 | async-start | bytes 786432 | tf_op jit(solution)/shard_map/all_to_all | solution.py:148
  122.5 9.3 %all-to-all-done.1 = bf16[16,12,768]{2,1,0:T(8,128)(2,1)S(1)} async-done(((bf16[16,12,768]{2,1,0:T(8,128)(2,1)}), bf16[16,12,768]{2,1,0:T(8,128)(2,1)S(1)}, u32[]{:S(2)}, u32[]{:S(2)}) %all-to-all-start.1) | async-done | bytes 294944 | tf_op jit(solution)/shard_map/all_to_all | solution.py:148
  131.9 0.8 gather_fusion
  133.0 78.1 %reduce-scatter.5.cloned.1.call-done = f32[1,16,768]{2,1,0:T(8,128)} async-done(((f32[32,16,768]{2,1,0:T(8,128)}), f32[1,16,768]{2,1,0:T(8,128)}) %reduce-scatter.5.cloned.1.call-update) | async-done | bytes 49168 | tf_op jit(solution)/shard_map/reduce_scatter | solution.py:166
  211.1 1.5 fusion.37
  (80 shorter events, 3.4 us)
Async XLA Ops:
  7.2 25.2 %copy-start = (bf16[384,1536]{1,0:T(8,128)(2,1)S(1)}, bf16[384,1536]{1,0:T(8,128)(2,1)}, u32[]{:S(2)}) copy-start(bf16[384,1536]{1,0:T(8,128)(2,1)} %param.37) | copy-start | bytes 3538948
  7.2 7.8 %copy-start.1 = (bf16[16,1536]{1,0:T(8,128)(2,1)S(1)}, bf16[16,1536]{1,0:T(8,128)(2,1)}, u32[]{:S(2)}) copy-start(bf16[16,1536]{1,0:T(8,128)(2,1)} %param.24) | copy-start | bytes 147460
  7.2 7.8 %copy-start.7 = (f32[1536]{0:T(1024)S(1)}, f32[1536]{0:T(1024)}, u32[]{:S(2)}) copy-start(f32[1536]{0:T(1024)} %param.26) | copy-start | bytes 18436
  7.2 7.8 %copy-start.8 = (bf16[96,384]{1,0:T(8,128)(2,1)S(1)}, bf16[96,384]{1,0:T(8,128)(2,1)}, u32[]{:S(2)}) copy-start(bf16[96,384]{1,0:T(8,128)(2,1)} %param.34) | copy-start | bytes 221188
  7.2 7.8 %copy-start.5 = (bf16[1536,96]{0,1:T(8,128)(2,1)S(1)}, bf16[1536,96]{0,1:T(8,128)(2,1)}, u32[]{:S(2)}) copy-start(bf16[1536,96]{0,1:T(8,128)(2,1)} %param.33) | copy-start | bytes 884740
  7.2 7.8 %copy-start.13 = (f32[384]{0:T(512)S(1)}, f32[384]{0:T(512)}, u32[]{:S(2)}) copy-start(f32[384]{0:T(512)} %param.35) | copy-start | bytes 4612
  7.2 8.4 %copy-start.9 = (bf16[96,384]{1,0:T(8,128)(2,1)S(1)}, bf16[96,384]{1,0:T(8,128)(2,1)}, u32[]{:S(2)}) copy-start(bf16[96,384]{1,0:T(8,128)(2,1)} %param.31) | copy-start | bytes 221188
  7.2 8.4 %copy-start.6 = (bf16[1536,96]{0,1:T(8,128)(2,1)S(1)}, bf16[1536,96]{0,1:T(8,128)(2,1)}, u32[]{:S(2)}) copy-start(bf16[1536,96]{0,1:T(8,128)(2,1)} %param.30) | copy-start | bytes 884740
  7.3 8.4 %copy-start.14 = (f32[384]{0:T(512)S(1)}, f32[384]{0:T(512)}, u32[]{:S(2)}) copy-start(f32[384]{0:T(512)} %param.32) | copy-start | bytes 4612
  7.3 109.7 %reduce-scatter.3.cloned.1.call-start = ((), (), s32[]{:S(2)}) async-start(), calls=%async_computation.4 | async-start | bytes 884736 | tf_op jit(solution)/shard_map/reduce_scatter | solution.py:144
  16.3 16.0 %copy-start.15 = (f32[384]{0:T(512)S(1)}, f32[384]{0:T(512)}, u32[]{:S(2)}) copy-start(f32[384]{0:T(512)} %param.36) | copy-start | bytes 4612
  16.3 21.0 %copy-start.11 = (f32[1536]{0:T(1024)S(1)}, f32[1536]{0:T(1024)}, u32[]{:S(2)}) copy-start(f32[1536]{0:T(1024)} %param.38) | copy-start | bytes 18436
  37.0 31.7 %copy-start.4 = (bf16[1,1536,192]{1,2,0:T(8,128)(2,1)S(1)}, bf16[1,1536,192]{1,2,0:T(8,128)(2,1)}, u32[]{:S(2)}) copy-start(bf16[1,1536,192]{1,2,0:T(8,128)(2,1)} %param.41) | copy-start | bytes 1769476
  68.7 45.6 %copy-start.2 = (bf16[1536,192]{0,1:T(8,128)(2,1)S(1)}, bf16[1536,192]{0,1:T(8,128)(2,1)}, u32[]{:S(2)}) copy-start(bf16[1536,192]{0,1:T(8,128)(2,1)} %param.44) | copy-start | bytes 1769476
  69.1 45.7 %copy-start.16 = (bf16[1536,192]{0,1:T(8,128)(2,1)S(1)}, bf16[1536,192]{0,1:T(8,128)(2,1)}, u32[]{:S(2)}) copy-start(bf16[1536,192]{0,1:T(8,128)(2,1)} %param.45) | copy-start | bytes 1769476
  72.0 43.3 %copy-start.3 = (bf16[192,1536]{1,0:T(8,128)(2,1)S(1)}, bf16[192,1536]{1,0:T(8,128)(2,1)}, u32[]{:S(2)}) copy-start(bf16[192,1536]{1,0:T(8,128)(2,1)} %param.46) | copy-start | bytes 1769476
  72.1 139.0 %reduce-scatter.5.cloned.1.call-start = ((), (), s32[]{:S(2)}) async-start(), calls=%async_computation.5 | async-start | bytes 1622016 | tf_op jit(solution)/shard_map/reduce_scatter | solution.py:166
  114.8 2.1 copy-start.10
  115.2 7.2 %copy-start.12 = (bf16[1536]{0:T(1024)(128)(2,1)S(1)}, bf16[1536]{0:T(1024)(128)(2,1)}, u32[]{:S(2)}) copy-start(bf16[1536]{0:T(1024)(128)(2,1)} %param.47) | copy-start | bytes 9220
  118.7 13.2 %all-to-all-start.1 = ((bf16[16,12,768]{2,1,0:T(8,128)(2,1)}), bf16[16,12,768]{2,1,0:T(8,128)(2,1)S(1)}, u32[]{:S(2)}, u32[]{:S(2)}) async-start(bf16[16,12,768]{2,1,0:T(8,128)(2,1)} %reshape.143), calls=%async_computation.2 | async-start | bytes 786432 | tf_op jit(solution)/shard_map/all_to_all | solution.py:148
Sparse Core Ops, SparseCore 0:
  72.2 5.7 reduce-scatter.2
  117.0 94.0 reduce-scatter.4
where the time goes:
time: 220 us; the launch traced here: 219 us
  waiting for transfers between devices  87.5 us (40%)
  blocking collectives  75.7 us (34%)
  other arithmetic  20.2 us (9%)
  between operations  14.5 us (7%)
  matrix products  11.7 us (5%)
  local copies, waits for them, and re-layouts  6.16 us (3%)
  starting transfers between devices  3.63 us (2%)
    reduce_scatter x1, waiting for transfers between devices, shards(): lax.psum_scatter(term, ('ep', 'tp'), scatter_dimension=0, tiled=True)[0]  78.1 us
    all_gather x1, blocking collectives, shards(): piece = lax.all_gather(mid, 'ep', axis=0, tiled=True)  42.2 us
    all_to_all x1, blocking collectives, shards(): lax.all_to_all(send, 'ep', split_axis=0, concat_axis=0, tiled=True)  29.6 us
    mul x1, other arithmetic, mixer_core(): removed[..., None] * (unit_key * learn_rate)[:, :, None, :]  15.7 us
    all_to_all x1, waiting for transfers between devices, shards(): back = lax.all_to_all(result, 'ep', split_axis=0, concat_axis=0, tiled=True)  9.34 us
    dot_general x3, matrix products, project(): product = jnp.dot(normed, weight, preferred_element_type=jnp.float32)  4.89 us
  transfers between devices with their start and end apart: 3, of which 2 were waited for; matrix products, arithmetic and copies ran while one was open for 3% of the time, Pallas kernels for 0%

commit v1 on v0

v1 whole, which is shorter than its diff:
```python
import functools

import jax
import jax.numpy as jnp
from jax import lax
from jax.experimental import pallas as pl
from jax.experimental.pallas import tpu as pltpu
from jax.sharding import PartitionSpec as P

MESH = pl.DeviceIdType.MESH
F32 = jnp.float32
BF16 = jnp.bfloat16
ANY = pl.BlockSpec(memory_space=pl.ANY)
VMEM = pl.BlockSpec(memory_space=pltpu.VMEM)


def dot(a, b):
    return jnp.dot(a, b, preferred_element_type=F32)


def dot_t(a, b):
    return lax.dot_general(a, b, (((1,), (1,)), ((), ())), preferred_element_type=F32)


def sigmoid(x):
    return 1.0 / (1.0 + jnp.exp(-x))


def front_kernel(
    tok, state, gain, wq, wk, wv, dd, du, db, rd, ru, rb, hg, ow,
    part, new_state,
    q_v, k_v, v_v, ow_v, st, sto, vec, reads, wsem, isem, osem,
):
    rows, heads, size = st.shape[0], st.shape[1], st.shape[2]
    weights = [
        pltpu.make_async_copy(src, dst, wsem.at[i])
        for i, (src, dst) in enumerate(((wk, k_v), (wq, q_v), (wv, v_v), (ow, ow_v)))
    ]
    for copy in weights[:3]:
        copy.start()

    def state_in(r):
        return pltpu.make_async_copy(state.at[r], st.at[r], isem.at[r])

    def state_out(r):
        return pltpu.make_async_copy(sto.at[r], new_state.at[r], osem.at[r])

    for r in range(rows):
        state_in(r).start()
    weights[3].start()

    x = tok[...].astype(F32)
    scale = lax.rsqrt(jnp.mean(x * x, axis=-1, keepdims=True) + 1e-06)
    normed = (x * scale * gain[...][None, :]).astype(BF16)
    low = jnp.tanh(dot_t(normed, dd[...])).astype(BF16)
    decay = jnp.exp(-0.6065306597126334 * sigmoid(db[...][None, :] + dot(low, du[...])))
    rlow = dot_t(normed, rd[...]).astype(BF16)
    rate = sigmoid(rb[...][None, :] + dot(rlow, ru[...]))
    weights[0].wait()
    key = dot(normed, k_v[...]).astype(BF16).astype(F32)
    weights[1].wait()
    rec = dot(normed, q_v[...]).astype(BF16).astype(F32)
    weights[2].wait()
    val = dot(normed, v_v[...]).astype(BF16).astype(F32)
    for h in range(heads):
        at = slice(h * size, (h + 1) * size)
        kh = key[:, at]
        unit = kh * lax.rsqrt(jnp.sum(kh * kh, axis=-1, keepdims=True) + 1e-06)
        vec[0, h] = unit
        vec[1, h] = decay[:, at]
        vec[2, h] = unit * rate[:, at]
        vec[3, h] = kh
        vec[4, h] = rec[:, at]
        vec[5, h] = val[:, at]

    eye = lax.broadcasted_iota(jnp.int32, (size, size), 0) == lax.broadcasted_iota(
        jnp.int32, (size, size), 1
    )

    def step(r, carry):
        state_in(r).wait()
        for h in range(heads):
            unit, dec, ul, kh, qh, vh = [vec[j, h, pl.ds(r, 1), :] for j in range(6)]
            s = st[r, h]
            removed = jnp.sum(s * unit, axis=-1, keepdims=True)
            vcol = jnp.sum(jnp.where(eye, vh, 0.0), axis=-1, keepdims=True)
            new = s * dec - removed * ul + vcol * kh
            sto[r, h] = new
            read = jnp.sum(new * qh, axis=-1, keepdims=True)
            reads[h, pl.ds(r, 1), :] = jnp.sum(jnp.where(eye, read, 0.0), axis=0, keepdims=True)
        state_out(r).start()
        return carry

    lax.fori_loop(0, rows, step, 0)
    weights[3].wait()
    total = None
    for h in range(heads):
        at = slice(h * size, (h + 1) * size)
        read = reads[h]
        read = read - jnp.mean(read, axis=-1, keepdims=True)
        spread = jnp.mean(read * read, axis=-1, keepdims=True)
        mixed = (read * lax.rsqrt(spread + 0.00064) * hg[...][None, :][:, at]).astype(BF16)
        term = dot(mixed, ow_v[h * size : (h + 1) * size, :])
        total = term if total is None else total + term
    part[...] = total.astype(BF16)

    def drain(r, carry):
        state_out(r).wait()
        return carry

    lax.fori_loop(0, rows, drain, 0)


def back_kernel(
    count, plane,
    tok, part, gain, ids, scores, blend_vec, eg, eu, ed, dg, du, dn,
    out,
    eg_v, eu_v, ed_v, dg_v, du_v, dn_v, prx, gbuf, res, hid_e, hid_d, own, ds2, dr2, r1s, r1r, r2s, r2r,
    wsem, xs, xr, agr, zs, ps, fs, fr, d2s, d2r, s1, r1, s2, r2,
):
    e = lax.axis_index("ep")
    t = lax.axis_index("tp")
    other = 1 - t
    depth = count // plane
    z, p = e // plane, e % plane
    seqs, width = tok.shape
    half = width // 2
    tail = gbuf.shape[3] - half
    top = ids.shape[0]

    barrier = pltpu.get_barrier_semaphore()

    def greet(device):
        pl.semaphore_signal(barrier, inc=1, device_id=device, device_id_type=MESH)

    def at_z(dz):
        return (z + dz) % depth

    def at_p(dp):
        return (p + dp) % plane

    greet((e, other))
    for dz in range(1, depth):
        greet((at_z(dz) * plane + p, t))
    for dp in range(1, plane):
        greet((z * plane + at_p(dp), t))

    weights = [
        pltpu.make_async_copy(src, dst, wsem.at[i])
        for i, (src, dst) in enumerate(
            ((eg.at[0], eg_v), (eu.at[0], eu_v), (dg, dg_v), (du, du_v), (ed.at[0], ed_v), (dn, dn_v))
        )
    ]
    for copy in weights:
        copy.start()

    def remote(src, dst, send, recv, device):
        return pltpu.make_async_remote_copy(
            src_ref=src, dst_ref=dst, send_sem=send, recv_sem=recv,
            device_id=device, device_id_type=MESH,
        )

    lanes = lax.broadcasted_iota(jnp.int32, (seqs, tail), 1)
    score = scores[...]
    share = score / jnp.sum(score, axis=0, keepdims=True) * 2.5
    id_all = ids[...].astype(F32)
    eye = lax.broadcasted_iota(jnp.int32, (seqs, seqs), 0) == lax.broadcasted_iota(
        jnp.int32, (seqs, seqs), 1
    )

    def column(row):
        return jnp.sum(jnp.where(eye, row, 0.0), axis=1, keepdims=True)

    table = jnp.zeros((seqs, tail), F32)
    for k in range(top):
        named = lanes.astype(F32) == column(id_all[k : k + 1, :])
        table = table + jnp.where(named, column(share[k : k + 1, :]), 0.0)

    pl.semaphore_wait(barrier, 1 + (depth - 1) + (plane - 1))
    swap = remote(part, prx, xs, xr, (e, other))
    swap.start()
    token_f = tok[...].astype(F32)
    swap.wait()
    resid = (token_f + (part[...].astype(F32) + prx[...].astype(F32))).astype(BF16).astype(F32)
    res[0] = resid[:, :half]
    res[1] = resid[:, half:]
    scale = lax.rsqrt(jnp.mean(resid * resid, axis=-1, keepdims=True) + 1e-06)
    mid = (resid * scale * gain[...][None, :]).astype(BF16)
    gated = jnp.sum(mid.astype(F32) * blend_vec[...][None, :].astype(F32), axis=-1, keepdims=True)
    table = jnp.where(lanes == count, sigmoid(gated), table)
    high = table.astype(BF16)
    gbuf[0, e, :, :half] = mid[:, :half]
    gbuf[1, e, :, :half] = mid[:, half:]
    gbuf[0, e, :, half:] = high
    gbuf[1, e, :, half:] = (table - high.astype(F32)).astype(BF16)

    def block(o, send, device):
        return remote(gbuf.at[t, o], gbuf.at[t, o], send, agr.at[o], device)

    def forward(o):
        return remote(gbuf.at[t, o], gbuf.at[t, o], fs.at[o], fr.at[o], (e, other))

    for dz in range(1, depth):
        block(e, zs.at[dz], (at_z(dz) * plane + p, t)).start()
    for dp in range(1, plane):
        block(e, ps.at[0, dp], (z * plane + at_p(dp), t)).start()
    for dz in range(1, depth):
        o = at_z(dz) * plane + p
        block(o, zs.at[dz], (e, other)).wait_recv()
        for dp in range(1, plane):
            block(o, ps.at[dz, dp], (z * plane + at_p(dp), t)).start()
        forward(o).start()
    for dz in range(depth):
        for dp in range(1, plane):
            o = at_z(dz) * plane + at_p(dp)
            block(o, zs.at[0], (e, other)).wait_recv()
            forward(o).start()
    for dz in range(depth):
        for dp in range(plane):
            if dz or dp:
                o = at_z(dz) * plane + at_p(dp)
                remote(
                    gbuf.at[other, o], gbuf.at[other, o], fs.at[o], fr.at[o], (e, other)
                ).wait_recv()
    for copy in weights:
        copy.wait()

    group = min(count, 16)
    size = group * seqs

    def hidden(c, carry):
        where = pl.ds(c * group, group)
        x0 = gbuf[0, where, :, :half].reshape(size, half)
        x1 = gbuf[1, where, :, :half].reshape(size, half)
        tab = gbuf[0, where, :, half:].astype(F32) + gbuf[1, where, :, half:].astype(F32)
        tab = tab.reshape(size, tail)
        lane = lax.broadcasted_iota(jnp.int32, (size, tail), 1)

        def pick(slot):
            return jnp.sum(jnp.where(lane == slot, tab, 0.0), axis=1, keepdims=True)

        def branch(gate, up, factor):
            g = dot_t(x0, gate[:, :half]) + dot_t(x1, gate[:, half:])
            u = dot_t(x0, up[:, :half]) + dot_t(x1, up[:, half:])
            return (g * sigmoid(g) * u * factor).astype(BF16).reshape(group, seqs, -1)

        hid_e[where] = branch(eg_v, eu_v, pick(e))
        hid_d[where] = branch(dg_v, du_v, pick(count))
        return carry

    lax.fori_loop(0, count // group, hidden, 0)

    def to_partner(c):
        return remote(ds2.at[c], dr2.at[c], d2s.at[c], d2r.at[c], (e, other))

    mine_at = pl.ds(pl.multiple_of(t * half, 128), half)
    theirs_at = pl.ds(pl.multiple_of(other * half, 128), half)

    def down(i, carry):
        c = at_z(i + 1)
        he = hid_e[pl.ds(c * plane, plane)].reshape(plane * seqs, -1)
        hd = hid_d[pl.ds(c * plane, plane)].reshape(plane * seqs, -1)
        theirs = dot(he, ed_v[:, theirs_at]) + dot(hd, dn_v[:, theirs_at])
        ds2[c] = theirs.astype(BF16).reshape(plane, seqs, half)
        to_partner(c).start()
        mine = dot(he, ed_v[:, mine_at]) + dot(hd, dn_v[:, mine_at])
        own[c] = mine.reshape(plane, seqs, half)
        return carry

    lax.fori_loop(0, depth, down, 0)

    def in_plane(c, dp):
        q = at_p(dp)
        return remote(r1s.at[c, q], r1r.at[c, p], s1.at[c, q], r1.at[c, p], (z * plane + q, t))

    def spread(i, carry):
        c = at_z(i + 1)
        to_partner(c).wait_recv()
        total = own[c] + dr2[c].astype(F32)
        own[c] = total
        r1s[c] = total.astype(BF16)
        for dp in range(1, plane):
            in_plane(c, dp).start()
        return carry

    lax.fori_loop(0, depth, spread, 0)

    def along_z(c):
        return remote(r2s.at[c], r2r.at[z], s2.at[c], r2.at[z], (c * plane + p, t))

    acc = None
    for i in range(depth):
        c = at_z(i + 1)
        acc = own[c, p]
        for dp in range(1, plane):
            q = at_p(dp)
            remote(r1s.at[c, q], r1r.at[c, q], s1.at[c, q], r1.at[c, q], (e, other)).wait_recv()
            acc = acc + r1r[c, q].astype(F32)
        if i < depth - 1:
            r2s[c] = acc.astype(BF16)
            along_z(c).start()
    for i in range(depth - 1):
        c = at_z(i + 1)
        remote(r2s.at[c], r2r.at[c], s2.at[c], r2.at[c], (e, other)).wait_recv()
        acc = acc + r2r[c].astype(F32)
    out[...] = (res[t] + acc).astype(BF16)

    for dz in range(1, depth):
        block(e, zs.at[dz], (at_z(dz) * plane + p, t)).wait_send()
        along_z(at_z(dz)).wait_send()
    for dz in range(depth):
        to_partner(at_z(dz)).wait_send()
        for dp in range(plane):
            o = at_z(dz) * plane + at_p(dp)
            if dp:
                block(at_z(dz) * plane + p, ps.at[dz, dp], (z * plane + at_p(dp), t)).wait_send()
                in_plane(at_z(dz), dp).wait_send()
            if dz or dp:
                forward(o).wait_send()


def shards(
    tokens, prior_state, first_gain, query_weight, key_weight, value_weight,
    decay_down, decay_up, decay_base, rate_down, rate_up, rate_base, head_gain,
    out_weight, mid_gain, route_ids, route_weights, expert_gate, expert_up, expert_down,
    dense_gate, dense_up, dense_down, blend_vector,
):
    count = lax.axis_size("ep")
    assert lax.axis_size("tp") == 2
    seqs, width = tokens.shape
    half = width // 2
    heads, size = prior_state.shape[1], prior_state.shape[2]
    inner = heads * size
    dma = pltpu.SemaphoreType.DMA
    part, new_state = pl.pallas_call(
        front_kernel,
        name="front",
        out_shape=(
            jax.ShapeDtypeStruct((seqs, width), BF16),
            jax.ShapeDtypeStruct(prior_state.shape, F32),
        ),
        in_specs=[VMEM, ANY, VMEM, ANY, ANY, ANY] + [VMEM] * 7 + [ANY],
        out_specs=(VMEM, ANY),
        scratch_shapes=[
            pltpu.VMEM((width, inner), BF16),
            pltpu.VMEM((width, inner), BF16),
            pltpu.VMEM((width, inner), BF16),
            pltpu.VMEM((inner, width), BF16),
            pltpu.VMEM(prior_state.shape, F32),
            pltpu.VMEM(prior_state.shape, F32),
            pltpu.VMEM((6, heads, seqs, size), F32),
            pltpu.VMEM((heads, seqs, size), F32),
            dma((4,)),
            dma((seqs,)),
            dma((seqs,)),
        ],
        compiler_params=pltpu.CompilerParams(vmem_limit_bytes=67043328),
    )(
        tokens, prior_state, first_gain, query_weight, key_weight, value_weight,
        decay_down.T, decay_up, decay_base, rate_down.T, rate_up, rate_base, head_gain, out_weight,
    )

    plane = 1
    while (plane * 2) ** 2 <= count and count % (plane * 2) == 0:
        plane *= 2
    depth = count // plane
    fe = expert_gate.shape[2]
    fd = dense_gate.shape[1]
    tail = -(-(count + 1) // 128) * 128
    mixed = pl.pallas_call(
        functools.partial(back_kernel, count, plane),
        name="back",
        out_shape=jax.ShapeDtypeStruct((seqs, half), BF16),
        in_specs=[VMEM] * 6 + [ANY] * 6,
        out_specs=VMEM,
        scratch_shapes=[
            pltpu.VMEM((fe, width), BF16),
            pltpu.VMEM((fe, width), BF16),
            pltpu.VMEM((fe, width), BF16),
            pltpu.VMEM((fd, width), BF16),
            pltpu.VMEM((fd, width), BF16),
            pltpu.VMEM((fd, width), BF16),
            pltpu.VMEM((seqs, width), BF16),
            pltpu.VMEM((2, count, seqs, half + tail), BF16),
            pltpu.VMEM((2, seqs, half), F32),
            pltpu.VMEM((count, seqs, fe), BF16),
            pltpu.VMEM((count, seqs, fd), BF16),
            pltpu.VMEM((depth, plane, seqs, half), F32),
            pltpu.VMEM((depth, plane, seqs, half), BF16),
            pltpu.VMEM((depth, plane, seqs, half), BF16),
            pltpu.VMEM((depth, plane, seqs, half), BF16),
            pltpu.VMEM((depth, plane, seqs, half), BF16),
            pltpu.VMEM((depth, seqs, half), BF16),
            pltpu.VMEM((depth, seqs, half), BF16),
            dma((6,)),
            dma,
            dma,
            dma((count,)),
            dma((depth,)),
            dma((depth, plane)),
            dma((count,)),
            dma((count,)),
            dma((depth,)),
            dma((depth,)),
            dma((depth, plane)),
            dma((depth, plane)),
            dma((depth,)),
            dma((depth,)),
        ],
        compiler_params=pltpu.CompilerParams(
            collective_id=0, has_side_effects=True, vmem_limit_bytes=67043328
        ),
    )(
        tokens, part, mid_gain, route_ids.T, route_weights.T, blend_vector,
        jnp.swapaxes(expert_gate, 1, 2), jnp.swapaxes(expert_up, 1, 2), expert_down,
        dense_gate.T, dense_up.T, dense_down,
    )
    return (mixed, new_state)


def solution(mesh):
    in_specs = (
        P("ep", None),
        P("ep", "tp", None, None),
        P(),
        P(None, "tp"),
        P(None, "tp"),
        P(None, "tp"),
        P(),
        P(None, "tp"),
        P("tp"),
        P(),
        P(None, "tp"),
        P("tp"),
        P("tp"),
        P("tp", None),
        P(),
        P("ep", None),
        P("ep", None),
        P("ep", None, "tp"),
        P("ep", None, "tp"),
        P("ep", "tp", None),
        P(None, ("ep", "tp")),
        P(None, ("ep", "tp")),
        P(("ep", "tp"), None),
        P(),
    )
    out_specs = (P("ep", "tp"), P("ep", "tp", None, None))
    return jax.shard_map(shards, mesh=mesh, in_specs=in_specs, out_specs=out_specs, check_vma=False)
```

time: 220 us -> 44.8 us (0.20)
  waiting for transfers between devices: 87.5 us -> 0 us
  blocking collectives: 75.7 us -> 0 us
  Pallas kernels: 0 us -> 42.5 us
  other arithmetic: 20.2 us -> 0 us
  between operations: 14.5 us -> 0.65 us
  matrix products: 11.7 us -> 0 us
  local copies, waits for them, and re-layouts: 6.16 us -> 1.35 us
  starting transfers between devices: 3.63 us -> 0 us
    reduce_scatter x2 -> x0, waiting for transfers between devices: 78.1 us -> none  [the longest x1 78.1 us: shards(): lax.psum_scatter(term, ('ep', 'tp'), scatter_dimension=0, tiled=True)[0]]
    pallas_call x0 -> x2, Pallas kernels: none -> 42.5 us  [the longest x1 31.4 us: shards(): pl.pallas_call(functools.partial(back_kernel, count, plane), name='back',...]
    all_gather x1 -> x0, blocking collectives: 42.2 us -> none  [shards(): piece = lax.all_gather(mid, 'ep', axis=0, tiled=True)]
    all_to_all x1 -> x0, blocking collectives: 29.6 us -> none  [shards(): lax.all_to_all(send, 'ep', split_axis=0, concat_axis=0, tiled=True)]
    mul x5 -> x0, other arithmetic: 16.7 us -> none  [the longest x1 15.7 us: mixer_core(): removed[..., None] * (unit_key * learn_rate)[:, :, None, :]]
    dot_general x12 -> x0, matrix products: 11.7 us -> none  [the longest x3 4.89 us: project(): product = jnp.dot(normed, weight, preferred_element_type=jnp.float32)]
    all_to_all x1 -> x0, waiting for transfers between devices: 9.34 us -> none  [shards(): back = lax.all_to_all(result, 'ep', split_axis=0, concat_axis=0, tiled=True)]
    psum x1 -> x0, blocking collectives: 3.85 us -> none  [shards(): lax.psum(partial_value.astype(jnp.bfloat16), 'tp').astype(jnp.float32)]
  transfers between devices with their start and end apart: 3 -> 0, of which waited for: 2 -> 0; matrix products, arithmetic and copies ran while one was open for 3% -> 0% of each run, Pallas kernels for 0% -> 0%
where the time goes in v1:
time: 44.8 us; the launch traced here: 44.5 us
  Pallas kernels  42.5 us (95%)
  local copies, waits for them, and re-layouts  1.35 us (3%)
  between operations  0.65 us (1%)
    pallas_call x1, Pallas kernels, shards(): pl.pallas_call(functools.partial(back_kernel, count, plane), name='back',...  31.4 us
    pallas_call x1, Pallas kernels, shards(): pl.pallas_call(front_kernel, name='front', out_shape=(jax.ShapeDtypeStruc...  11.1 us
    unnamed x1, local copies, waits for them, and re-layouts  1.35 us

profile of v1, /device:TPU:0, one launch (start us, length us, event | category | flops | bytes accessed | tf_op | source)
XLA Modules:
  0.0 44.5 jit_solution(15151455549710541821)
XLA Ops:
  0.6 11.1 %front.1 = (bf16[16,1536]{1,0:T(8,128)(2,1)}, f32[16,6,64,64]{3,2,1,0:T(8,128)}) custom-call(bf16[16,1536]{1,0:T(8,128)(2,1)} %tok.3, f32[16,6,64,64]{3,2,1,0:T(8,128)} %state.1, f32[1536]{0:T(1024)} %gain.2, bf16[1536,384]{1,0:T(8,128)(2,1)} %wq.1, bf16[1536,384]{1,0:T(8,128)(2,1)} %wk.1, bf16[1536,384]{1,0:T(8,128)(2,1)} %wv.1, bf16[96,1536]{1,0:T(8,128)(2,1)} %bitcast.12, ...), custom_call_target="tpu_custom_call" | custom-call | tf_op jit(solution)/shard_map/front/pallas_call | solution.py:335
  11.8 31.4 %back.1 = bf16[16,768]{1,0:T(8,128)(2,1)} custom-call(bf16[16,1536]{1,0:T(8,128)(2,1)} %tok.3, bf16[16,1536]{1,0:T(8,128)(2,1)} %get-tuple-element.4.part, f32[1536]{0:T(1024)} %gain.3, s32[6,16]{1,0:T(8,128)} %bitcast.14, f32[6,16]{1,0:T(8,128)} %bitcast.15, bf16[1536]{0:T(1024)(128)(2,1)} %blend_vec.1, bf16[1,192,1536]{2,1,0:T(8,128)(2,1)} %bitcast.8, ...), custom_call_target="tpu_custom_call" | custom-call | tf_op jit(solution)/shard_map/back/pallas_call | solution.py:370
  43.2 1.3 %copy.27 = bf16[16,768]{1,0:T(8,128)(2,1)} copy(bf16[16,768]{1,0:T(8,128)(2,1)} %back.1) | data formatting | bytes 49152

commit v2 on v1

--- a/solution.py
+++ b/solution.py
@@ -77,21 +77,29 @@
         jnp.int32, (size, size), 1
     )
 
-    def step(r, carry):
-        state_in(r).wait()
-        for h in range(heads):
-            unit, dec, ul, kh, qh, vh = [vec[j, h, pl.ds(r, 1), :] for j in range(6)]
-            s = st[r, h]
-            removed = jnp.sum(s * unit, axis=-1, keepdims=True)
-            vcol = jnp.sum(jnp.where(eye, vh, 0.0), axis=-1, keepdims=True)
-            new = s * dec - removed * ul + vcol * kh
-            sto[r, h] = new
-            read = jnp.sum(new * qh, axis=-1, keepdims=True)
-            reads[h, pl.ds(r, 1), :] = jnp.sum(jnp.where(eye, read, 0.0), axis=0, keepdims=True)
-        state_out(r).start()
+    unity = jnp.where(eye, 1.0, 0.0).astype(BF16)
+
+    batch = 2
+
+    def step(i, carry):
+        for b in range(batch):
+            state_in(i * batch + b).wait()
+        for b in range(batch):
+            r = i * batch + b
+            for h in range(heads):
+                unit, dec, ul, kh, qh, vh = [vec[j, h, pl.ds(r, 1), :] for j in range(6)]
+                s = st[r, h]
+                removed = jnp.sum(s * unit, axis=-1, keepdims=True)
+                vcol = dot_t(unity, jnp.broadcast_to(vh, (size, size)).astype(BF16))
+                new = s * dec - removed * ul + vcol * kh
+                sto[r, h] = new
+                read = jnp.sum(new * qh, axis=-1, keepdims=True)
+                reads[h, pl.ds(r, 1), :] = jnp.sum(jnp.where(eye, read, 0.0), axis=0, keepdims=True)
+        for b in range(batch):
+            state_out(i * batch + b).start()
         return carry
 
-    lax.fori_loop(0, rows, step, 0)
+    lax.fori_loop(0, rows // batch, step, 0)
     weights[3].wait()
     total = None
     for h in range(heads):
@@ -138,6 +146,16 @@
 
     def at_p(dp):
         return (p + dp) % plane
+
+    def near(j):
+        low = j + (j - z + depth) // depth
+        flipped = depth - 1 - z
+        high = depth - 1 - (j + (j - flipped + depth) // depth)
+        return low + (2 * z) // depth * (high - low)
+
+    def far(i):
+        last = (i + 1) // depth
+        return (1 - last) * near((1 - last) * (depth - 2 - i)) + last * z
 
     greet((e, other))
     for dz in range(1, depth):
@@ -200,19 +218,19 @@
     def forward(o):
         return remote(gbuf.at[t, o], gbuf.at[t, o], fs.at[o], fr.at[o], (e, other))
 
-    for dz in range(1, depth):
-        block(e, zs.at[dz], (at_z(dz) * plane + p, t)).start()
+    for j in range(depth - 2, -1, -1):
+        block(e, zs.at[j + 1], (near(j) * plane + p, t)).start()
     for dp in range(1, plane):
         block(e, ps.at[0, dp], (z * plane + at_p(dp), t)).start()
     for dz in range(1, depth):
-        o = at_z(dz) * plane + p
+        o = near(dz - 1) * plane + p
         block(o, zs.at[dz], (e, other)).wait_recv()
         for dp in range(1, plane):
             block(o, ps.at[dz, dp], (z * plane + at_p(dp), t)).start()
         forward(o).start()
     for dz in range(depth):
         for dp in range(1, plane):
-            o = at_z(dz) * plane + at_p(dp)
+            o = (near(dz - 1) if dz else z) * plane + at_p(dp)
             block(o, zs.at[0], (e, other)).wait_recv()
             forward(o).start()
     for dz in range(depth):
@@ -257,7 +275,7 @@
     theirs_at = pl.ds(pl.multiple_of(other * half, 128), half)
 
     def down(i, carry):
-        c = at_z(i + 1)
+        c = far(i)
         he = hid_e[pl.ds(c * plane, plane)].reshape(plane * seqs, -1)
         hd = hid_d[pl.ds(c * plane, plane)].reshape(plane * seqs, -1)
         theirs = dot(he, ed_v[:, theirs_at]) + dot(hd, dn_v[:, theirs_at])
@@ -274,7 +292,7 @@
         return remote(r1s.at[c, q], r1r.at[c, p], s1.at[c, q], r1.at[c, p], (z * plane + q, t))
 
     def spread(i, carry):
-        c = at_z(i + 1)
+        c = far(i)
         to_partner(c).wait_recv()
         total = own[c] + dr2[c].astype(F32)
         own[c] = total
@@ -290,7 +308,7 @@
 
     acc = None
     for i in range(depth):
-        c = at_z(i + 1)
+        c = far(i)
         acc = own[c, p]
         for dp in range(1, plane):
             q = at_p(dp)
@@ -300,7 +318,7 @@
             r2s[c] = acc.astype(BF16)
             along_z(c).start()
     for i in range(depth - 1):
-        c = at_z(i + 1)
+        c = near(i)
         remote(r2s.at[c], r2r.at[c], s2.at[c], r2.at[c], (e, other)).wait_recv()
         acc = acc + r2r[c].astype(F32)
     out[...] = (res[t] + acc).astype(BF16)

time: 44.8 us -> 42.3 us (0.944)
  Pallas kernels: 42.5 us -> 40.1 us
    pallas_call x1, Pallas kernels: 11.1 us -> 8.88 us  [shards(): pl.pallas_call(front_kernel, name='front', out_shape=(jax.ShapeDtypeStruc...]
where the time goes in v2:
time: 42.3 us; the launch traced here: 42.1 us
  Pallas kernels  40.1 us (95%)
  local copies, waits for them, and re-layouts  1.35 us (3%)
  between operations  0.65 us (2%)
    pallas_call x1, Pallas kernels, shards(): pl.pallas_call(functools.partial(back_kernel, count, plane), name='back',...  31.2 us
    pallas_call x1, Pallas kernels, shards(): pl.pallas_call(front_kernel, name='front', out_shape=(jax.ShapeDtypeStruc...  8.88 us
    unnamed x1, local copies, waits for them, and re-layouts  1.35 us

profile of v2, /device:TPU:0, one launch (start us, length us, event | category | flops | bytes accessed | tf_op | source)
XLA Modules:
  0.0 42.1 jit_solution(8582314426063248024)
XLA Ops:
  0.6 8.9 %front.1 = (bf16[16,1536]{1,0:T(8,128)(2,1)}, f32[16,6,64,64]{3,2,1,0:T(8,128)}) custom-call(bf16[16,1536]{1,0:T(8,128)(2,1)} %tok.3, f32[16,6,64,64]{3,2,1,0:T(8,128)} %state.1, f32[1536]{0:T(1024)} %gain.2, bf16[1536,384]{1,0:T(8,128)(2,1)} %wq.1, bf16[1536,384]{1,0:T(8,128)(2,1)} %wk.1, bf16[1536,384]{1,0:T(8,128)(2,1)} %wv.1, bf16[96,1536]{1,0:T(8,128)(2,1)} %bitcast.12, ...), custom_call_target="tpu_custom_call" | custom-call | tf_op jit(solution)/shard_map/front/pallas_call | solution.py:353
  9.5 31.2 %back.1 = bf16[16,768]{1,0:T(8,128)(2,1)} custom-call(bf16[16,1536]{1,0:T(8,128)(2,1)} %tok.3, bf16[16,1536]{1,0:T(8,128)(2,1)} %get-tuple-element.4.part, f32[1536]{0:T(1024)} %gain.3, s32[6,16]{1,0:T(8,128)} %bitcast.14, f32[6,16]{1,0:T(8,128)} %bitcast.15, bf16[1536]{0:T(1024)(128)(2,1)} %blend_vec.1, bf16[1,192,1536]{2,1,0:T(8,128)(2,1)} %bitcast.8, ...), custom_call_target="tpu_custom_call" | custom-call | tf_op jit(solution)/shard_map/back/pallas_call | solution.py:388
  40.7 1.3 %copy.27 = bf16[16,768]{1,0:T(8,128)(2,1)} copy(bf16[16,768]{1,0:T(8,128)(2,1)} %back.1) | data formatting | bytes 49152
